TPU v7x, 32 devices: a whole 2x2x4 slice. The times are simulated.
32 devices in a mesh: sp: 8 (over z, core), tp: 4 (over y, x).
Axes of the slice: x: 2, y: 2, z: 4, core: 2. Of those that a mesh axis runs over, the one named last changes fastest.
Arguments:
- residual_in: bfloat16 [2048, 2048], P('sp'), may hold values from -3 to 3
- mix_gain: float32 [2048], replicated, may hold values from 0.1 to 1.9
- pool_weight: bfloat16 [512, 2048], P(None, 'tp'), may hold values from -0.5 to 0.5
- pool_scale: float32 [2048], P('tp'), may hold values from 0.1 to 1.9
- ffn_gain: float32 [2048], replicated, may hold values from 0.1 to 1.9
- route_ids: int32 [2048, 2], P('sp'), may hold values from 0 to 7, all different within a row; in each aligned block of 64 rows (0 to 63, 64 to 127, ...) at most 32 rows name the same one
- route_weights: float32 [2048, 2], P('sp'), may hold values from 0.1 to 1
- gate_weight: bfloat16 [8, 2048, 3584], P('sp', None, 'tp'), may hold values from -0.125 to 0.125
- up_weight: bfloat16 [8, 2048, 3584], P('sp', None, 'tp'), may hold values from -0.125 to 0.125
- down_weight: bfloat16 [8, 3584, 2048], P('sp', 'tp'), may hold values from -0.09375 to 0.09375
Outputs:
- layer_out: bfloat16 [2048, 2048], P('sp')
Inputs may be any that keep to these rules, and one draw needn't show every extreme that they name: `route_ids`: each row names 2 different experts; in each aligned block of 64 rows no expert is named by more than 32 rows, and some block has an expert named by exactly 32 rows.
All inputs are finite; a program needn't handle non-finite values.
Results may differ from a plain program's by a relative error of at most 0.0074.
Values may be sent and summed in bfloat16 or wider, within the bound.
A program may use at most 64 MiB of HBM per device.

v0:
```python
import jax
import jax.numpy as jnp
from jax import lax
from jax.sharding import PartitionSpec as P

GROUPS = 4
SPAN = 16
TOP_K = 2
EPS = 1e-06


def from_behind(value, axis, steps):
    count = lax.axis_size(axis)
    first, last = (max(0, -steps), min(count, count - steps))
    return lax.ppermute(value, axis, [(source, source + steps) for source in range(first, last)])


def rms_scale(values, gain):
    return values * lax.rsqrt(jnp.mean(values * values, axis=-1, keepdims=True) + EPS) * gain


def slot_table(chosen_ids, experts, capacity):
    flat_ids = chosen_ids.reshape(-1)
    matches = (flat_ids[:, None] == jnp.arange(experts, dtype=jnp.int32)[None, :]).astype(jnp.int32)
    before = jnp.cumsum(matches, axis=0) - matches
    slot_of = jnp.sum(before * matches, axis=1)
    target = flat_ids * capacity + slot_of
    return (target[:, None] == jnp.arange(experts * capacity, dtype=jnp.int32)[None, :]).astype(
        jnp.float32
    )


def shards(
    residual_in,
    mix_gain,
    pool_weight,
    pool_scale,
    ffn_gain,
    route_ids,
    route_weights,
    gate_weight,
    up_weight,
    down_weight,
):
    tp_count = lax.axis_size("tp")
    sp_count = lax.axis_size("sp")
    tp_index = lax.axis_index("tp")
    tok_count, width = residual_in.shape
    group_width = width // GROUPS
    col_count = pool_weight.shape[1]
    row_count = tok_count // tp_count
    capacity = 2 * TOP_K * row_count // sp_count
    group_index = tp_index * col_count // group_width
    window = jnp.power(2, group_index + 1)
    stream = residual_in.astype(jnp.float32)
    inverse = lax.rsqrt(jnp.mean(stream * stream, axis=-1, keepdims=True) + EPS)
    stream_group = lax.dynamic_slice_in_dim(stream, group_index * group_width, group_width, 1)
    gain_group = lax.dynamic_slice_in_dim(mix_gain, group_index * group_width, group_width, 0)
    normed_group = (stream_group * inverse * gain_group).astype(jnp.bfloat16)
    rim_rows = from_behind(normed_group[tok_count - SPAN :], "sp", 1)
    extended = jnp.concatenate([rim_rows, normed_group], axis=0).astype(jnp.float32)
    window_sum = jnp.zeros((tok_count, group_width), jnp.float32)
    for offset in range(SPAN):
        window_sum = window_sum + jnp.where(
            offset < window, extended[SPAN - offset : SPAN - offset + tok_count], 0.0
        )
    position = lax.axis_index("sp") * tok_count + jnp.arange(tok_count, dtype=jnp.int32)
    divisor = jnp.minimum(position + 1, window).astype(jnp.float32)
    pooled = (window_sum / divisor[:, None] - extended[SPAN:]).astype(jnp.bfloat16)
    mixed = (jnp.dot(pooled, pool_weight, preferred_element_type=jnp.float32) * pool_scale).astype(
        jnp.bfloat16
    )
    stream_own = lax.dynamic_slice_in_dim(stream, tp_index * row_count, row_count, 0)
    mixed_own = lax.all_to_all(mixed, "tp", split_axis=0, concat_axis=1, tiled=True)
    after_own = (stream_own + mixed_own.astype(jnp.float32)).astype(jnp.bfloat16)
    normed_own = rms_scale(after_own.astype(jnp.float32), ffn_gain).astype(jnp.bfloat16)
    ids_own = lax.dynamic_slice_in_dim(route_ids, tp_index * row_count, row_count, 0)
    table_own = slot_table(ids_own, sp_count, capacity)
    repeated = jnp.repeat(normed_own, TOP_K, axis=0)
    outgoing = lax.dot_general(
        table_own.astype(jnp.bfloat16),
        repeated,
        (((0,), (0,)), ((), ())),
        preferred_element_type=jnp.float32,
    )
    outgoing = outgoing.astype(jnp.bfloat16).reshape(sp_count, capacity, width)
    arrived = lax.all_to_all(outgoing, "sp", split_axis=0, concat_axis=0, tiled=True)
    piece = lax.all_gather(arrived, "tp", axis=0, tiled=True)
    flat_rows = piece.reshape(-1, width)
    gate_part = jnp.dot(flat_rows, gate_weight[0], preferred_element_type=jnp.float32)
    up_part = jnp.dot(flat_rows, up_weight[0], preferred_element_type=jnp.float32)
    hidden = (jax.nn.silu(gate_part) * up_part).astype(jnp.bfloat16)
    hidden_all = hidden.reshape(piece.shape[0], piece.shape[1], hidden.shape[1])
    hidden_flat = hidden_all.reshape(-1, hidden_all.shape[-1])
    term = jnp.dot(hidden_flat, down_weight[0], preferred_element_type=jnp.float32)
    summed = lax.psum_scatter(
        term.astype(jnp.bfloat16).astype(jnp.float32).astype(jnp.bfloat16),
        "tp",
        scatter_dimension=0,
        tiled=True,
    )
    expert_out = summed.reshape(sp_count, capacity, width)
    returned_rows = lax.all_to_all(expert_out, "sp", split_axis=0, concat_axis=0, tiled=True)
    weights_own = lax.dynamic_slice_in_dim(route_weights, tp_index * row_count, row_count, 0)
    weight_table = jnp.einsum(
        "rk,rkc->rc", weights_own, table_own.reshape(row_count, TOP_K, sp_count * capacity)
    )
    expert_mix = jnp.dot(
        weight_table,
        returned_rows.reshape(-1, width).astype(jnp.float32),
        precision=lax.Precision.HIGHEST,
    )
    out_own = (after_own.astype(jnp.float32) + expert_mix).astype(jnp.bfloat16)
    return lax.all_gather(out_own, "tp", axis=0, tiled=True)


def solution(mesh):
    placed = (
        P("sp", None),
        P(),
        P(None, "tp"),
        P("tp"),
        P(),
        P("sp", None),
        P("sp", None),
        P("sp", None, "tp"),
        P("sp", None, "tp"),
        P("sp", "tp", None),
    )
    return jax.shard_map(
        shards, mesh=mesh, in_specs=placed, out_specs=P("sp", None), check_vma=False
    )
```

profile of v0, /device:TPU:0, one launch (start us, length us, event | category | flops | bytes accessed | tf_op | source)
XLA Modules:
  0.0 247.7 jit_solution(884471469957618278)
XLA Ops:
  6.5 0.0 copy-start
  6.5 0.0 copy-start.3
  6.5 0.0 copy-start.7
  6.5 0.0 copy-start.1
  6.5 1.6 convert_element_type.65
  8.1 0.0 copy-done.1
  8.2 0.3 multiply_reduce_fusion
  8.5 0.8 dynamic_slice.17
  9.2 0.1 multiply_convert_fusion.1
  9.4 2.4 collective-permute-start
  11.8 0.0 copy-done.3
  11.8 0.1 constant_dynamic-slice_fusion
  11.9 0.1 copy.19
  12.0 0.1 eq.35
  12.1 0.1 fusion.38
  12.2 0.2 reduce_window_sum.11
  12.4 0.2 select_reduce_fusion
  12.6 0.0 collective-permute-done
  12.7 0.1 maximum_convert_fusion
  12.7 0.0 copy-done
  12.7 0.0 copy-done.7
  12.7 2.0 fusion.8
  14.7 0.0 copy-start.2
  14.7 4.7 %all-to-all-start = ((bf16[4,64,512]{2,1,0:T(8,128)(2,1)}), bf16[4,64,512]{2,1,0:T(8,128)(2,1)S(1)}, u32[]{:S(2)}, u32[]{:S(2)}) async-start(bf16[4,64,512]{2,1,0:T(8,128)(2,1)} %bitcast), calls=%async_computation | async-start | bytes 524288 | tf_op jit(solution)/shard_map/all_to_all | solution.py:74
  19.4 0.0 all-gather.3.cloned.1.call-start
  19.4 6.0 %all-to-all-done = bf16[4,64,512]{2,1,0:T(8,128)(2,1)S(1)} async-done(((bf16[4,64,512]{2,1,0:T(8,128)(2,1)}), bf16[4,64,512]{2,1,0:T(8,128)(2,1)S(1)}, u32[]{:S(2)}, u32[]{:S(2)}) %all-to-all-start) | async-done | bytes 262176 | tf_op jit(solution)/shard_map/all_to_all | solution.py:74
  25.5 0.2 fusion.9
  25.7 0.0 copy-done.2
  25.7 0.1 fusion.11
  25.8 0.3 broadcast_in_dim.32
  26.1 0.2 reshape.66
  26.3 0.5 convolution_convert_fusion.1
  26.9 33.2 %all_to_all.23 = bf16[8,32,2048]{2,1,0:T(8,128)(2,1)} all-to-all(bf16[8,32,2048]{2,1,0:T(8,128)(2,1)S(1)} %bitcast.33), channel_id=1, replica_groups=mesh['sp'=8,'tp'=4] {'sp'}, dimensions={0} | all-to-all | bytes 2097152 | tf_op jit(solution)/shard_map/all_to_all | solution.py:87
  60.0 0.0 all-gather.3.cloned.1.call-update
  60.1 0.0 reduce-scatter.2.cloned.1.call-start
  60.1 50.4 %all-gather.3.cloned.1.call-done = bf16[32,32,2048]{2,1,0:T(8,128)(2,1)} async-done(((bf16[8,32,2048]{2,1,0:T(8,128)(2,1)}), bf16[32,32,2048]{2,1,0:T(8,128)(2,1)}) %all-gather.3.cloned.1.call-update) | async-done | bytes 4194320 | tf_op jit(solution)/shard_map/all_gather | solution.py:88
  110.6 0.0 copy-start.4
  110.6 0.0 copy-start.5
  110.6 7.5 %fusion.1 = f32[1024,896]{1,0:T(8,128)S(1)} fusion(bf16[1024,2048]{1,0:T(8,128)(2,1)} %bitcast.36, bf16[1,2048,896]{2,1,0:T(8,128)(2,1)} %param.18), kind=kOutput, calls=%fused_computation.2 | convolution fusion | flops 3758096384 | bytes 11534336 | tf_op jit(solution)/shard_map/dot_general | solution.py:91
  118.1 0.0 copy-done.4
  118.1 0.0 copy-done.5
  118.1 0.0 copy-start.6
  118.1 4.7 %multiply_convert_fusion = bf16[1024,896]{1,0:T(8,128)(2,1)S(1)} fusion(f32[1024,896]{1,0:T(8,128)S(1)} %fusion.1, bf16[1024,2048]{1,0:T(8,128)(2,1)S(1)} %bitcast.37, bf16[1,2048,896]{2,1,0:T(8,128)(2,1)S(1)} %copy-done.5), kind=kOutput, calls=%fused_computation.6 | convolution fusion | flops 3763601408 | bytes 13369344 | tf_op jit(solution)/shard_map/dot_general | solution.py:90
  122.9 0.0 copy-done.6
  122.9 6.0 %convolution_convert_fusion = bf16[1024,2048]{1,0:T(8,128)(2,1)} fusion(bf16[1024,896]{1,0:T(8,128)(2,1)S(1)} %multiply_convert_fusion, bf16[1,896,2048]{2,1,0:T(8,128)(2,1)S(1)} %copy-done.6), kind=kOutput, calls=%fused_computation | convolution fusion | flops 3760193536 | bytes 9699328 | tf_op jit(solution)/shard_map/dot_general | solution.py:95
  128.9 0.0 reduce-scatter.2.cloned.1.call-update
  128.9 52.8 %reduce-scatter.2.cloned.1.call-done = bf16[256,2048]{1,0:T(8,128)(2,1)} async-done(((bf16[1024,2048]{1,0:T(8,128)(2,1)}), bf16[256,2048]{1,0:T(8,128)(2,1)}) %reduce-scatter.2.cloned.1.call-update) | async-done | bytes 1048592 | tf_op jit(solution)/shard_map/reduce_scatter | solution.py:96
  181.7 4.6 %all-to-all-start.2 = ((bf16[8,32,2048]{2,1,0:T(8,128)(2,1)}), bf16[8,32,2048]{2,1,0:T(8,128)(2,1)S(1)}, u32[]{:S(2)}, u32[]{:S(2)}) async-start(bf16[8,32,2048]{2,1,0:T(8,128)(2,1)} %bitcast.35), calls=%async_computation.3 | async-start | bytes 2097152 | tf_op jit(solution)/shard_map/all_to_all | solution.py:103
  186.3 0.0 all-gather.5.cloned.1.call-start
  186.3 0.1 reduce_sum.31
  186.5 0.8 dynamic-slice_bitcast_fusion
  187.2 0.1 copy.17
  187.4 0.3 fusion.30
  187.7 25.2 %all-to-all-done.2 = bf16[8,32,2048]{2,1,0:T(8,128)(2,1)S(1)} async-done(((bf16[8,32,2048]{2,1,0:T(8,128)(2,1)}), bf16[8,32,2048]{2,1,0:T(8,128)(2,1)S(1)}, u32[]{:S(2)}, u32[]{:S(2)}) %all-to-all-start.2) | async-done | bytes 1048608 | tf_op jit(solution)/shard_map/all_to_all | solution.py:103
  212.9 1.4 fusion.7
  214.2 0.0 all-gather.5.cloned.1.call-update
  214.3 24.6 %all-gather.5.cloned.1.call-done = bf16[256,2048]{1,0:T(8,128)(2,1)} async-done(((bf16[64,2048]{1,0:T(8,128)(2,1)}), bf16[256,2048]{1,0:T(8,128)(2,1)}) %all-gather.5.cloned.1.call-update) | async-done | bytes 1048592 | tf_op jit(solution)/shard_map/all_gather | solution.py:114
  238.9 2.3 copy.26
  (8 shorter events, 0.1 us)
Async XLA Ops:
  6.5 6.2 %copy-start = (bf16[512,512]{1,0:T(8,128)(2,1)S(1)}, bf16[512,512]{1,0:T(8,128)(2,1)}, u32[]{:S(2)}) copy-start(bf16[512,512]{1,0:T(8,128)(2,1)} %param.12) | copy-start | bytes 1572868
  6.5 5.3 %copy-start.3 = (s32[256,2]{0,1:T(2,128)S(1)}, s32[256,2]{0,1:T(2,128)}, u32[]{:S(2)}) copy-start(s32[256,2]{0,1:T(2,128)} %param.15) | copy-start | bytes 6148
  6.5 6.2 %copy-start.7 = (f32[512]{0:T(512)S(1)}, f32[512]{0:T(512)}, u32[]{:S(2)}) copy-start(f32[512]{0:T(512)} %param.13) | copy-start | bytes 6148
  6.5 1.6 copy-start.1
  9.4 3.3 %collective-permute-start = (bf16[16,512]{1,0:T(8,128)(2,1)S(1)}, bf16[16,512]{1,0:T(8,128)(2,1)S(1)}, u32[]{:S(2)}, u32[]{:S(2)}) collective-permute-start(bf16[16,512]{1,0:T(8,128)(2,1)S(1)} %slice.69), channel_id=1, source_target_pairs={{0,4},{4,8},{8,12},{12,16},{16,20},{20,24},{24,28},{1,5},{5,9},{9,... | collective-permute-start | bytes 49160 | tf_op jit(solution)/shard_map/ppermute | solution.py:15
  14.7 10.9 %copy-start.2 = (f32[2048]{0:T(1024)S(1)}, f32[2048]{0:T(1024)}, u32[]{:S(2)}) copy-start(f32[2048]{0:T(1024)} %param.14) | copy-start | bytes 24580
  14.7 10.6 %all-to-all-start = ((bf16[4,64,512]{2,1,0:T(8,128)(2,1)}), bf16[4,64,512]{2,1,0:T(8,128)(2,1)S(1)}, u32[]{:S(2)}, u32[]{:S(2)}) async-start(bf16[4,64,512]{2,1,0:T(8,128)(2,1)} %bitcast), calls=%async_computation | async-start | bytes 524288 | tf_op jit(solution)/shard_map/all_to_all | solution.py:74
  19.4 91.1 %all-gather.3.cloned.1.call-start = ((), (), s32[]{:S(2)}) async-start(), calls=%async_computation.4 | async-start | bytes 5242880 | tf_op jit(solution)/shard_map/all_gather | solution.py:88
  60.1 121.6 %reduce-scatter.2.cloned.1.call-start = ((), (), s32[]{:S(2)}) async-start(), calls=%async_computation.5 | async-start | bytes 5242880 | tf_op jit(solution)/shard_map/reduce_scatter | solution.py:96
  110.6 7.5 %copy-start.4 = (bf16[32,32,2048]{2,1,0:T(8,128)(2,1)S(1)}, bf16[32,32,2048]{2,1,0:T(8,128)(2,1)}, u32[]{:S(2)}) copy-start(bf16[32,32,2048]{2,1,0:T(8,128)(2,1)} %all-gather.3.cloned.1.call-done) | copy-start | bytes 12582916
  110.6 7.5 %copy-start.5 = (bf16[1,2048,896]{2,1,0:T(8,128)(2,1)S(1)}, bf16[1,2048,896]{2,1,0:T(8,128)(2,1)}, u32[]{:S(2)}) copy-start(bf16[1,2048,896]{2,1,0:T(8,128)(2,1)} %param.17) | copy-start | bytes 11010052
  118.1 4.8 %copy-start.6 = (bf16[1,896,2048]{2,1,0:T(8,128)(2,1)S(1)}, bf16[1,896,2048]{2,1,0:T(8,128)(2,1)}, u32[]{:S(2)}) copy-start(bf16[1,896,2048]{2,1,0:T(8,128)(2,1)} %param.19) | copy-start | bytes 11010052
  181.7 31.2 %all-to-all-start.2 = ((bf16[8,32,2048]{2,1,0:T(8,128)(2,1)}), bf16[8,32,2048]{2,1,0:T(8,128)(2,1)S(1)}, u32[]{:S(2)}, u32[]{:S(2)}) async-start(bf16[8,32,2048]{2,1,0:T(8,128)(2,1)} %bitcast.35), calls=%async_computation.3 | async-start | bytes 2097152 | tf_op jit(solution)/shard_map/all_to_all | solution.py:103
  186.3 52.6 %all-gather.5.cloned.1.call-start = ((), (), s32[]{:S(2)}) async-start(), calls=%async_computation.6 | async-start | bytes 1310720 | tf_op jit(solution)/shard_map/all_gather | solution.py:114
Sparse Core Ops, SparseCore 0:
  60.2 50.3 all-gather.2
  129.1 52.5 reduce-scatter.1
  214.4 24.4 all-gather.4
where the time goes:
time: 248 us
  waiting for transfers between devices  159 us (64%)
  blocking collectives  33.2 us (13%)
  matrix products  22.5 us (9%)
  between operations  13.4 us (5%)
  starting transfers between devices  11.7 us (5%)
  local copies, waits for them, and re-layouts  5 us (2%)
  other arithmetic  2.84 us (1%)
    reduce_scatter x1, waiting for transfers between devices, shards(): lax.psum_scatter(term.astype(jnp.bfloat16).astype(jnp.float32).astype(jnp...  52.8 us
    all_gather x1, waiting for transfers between devices, shards(): piece = lax.all_gather(arrived, 'tp', axis=0, tiled=True)  50.4 us
    all_to_all x1, blocking collectives, shards(): lax.all_to_all(outgoing, 'sp', split_axis=0, concat_axis=0, tiled=True)  33.2 us
    all_to_all x1, waiting for transfers between devices, shards(): lax.all_to_all(expert_out, 'sp', split_axis=0, concat_axis=0, tiled=True)  25.2 us
    all_gather x1, waiting for transfers between devices, shards(): return lax.all_gather(out_own, 'tp', axis=0, tiled=True)  24.6 us
    dot_general x1, matrix products, shards(): jnp.dot(flat_rows, up_weight[0], preferred_element_type=jnp.float32)  7.49 us
    dot_general x1, matrix products, shards(): jnp.dot(hidden_flat, down_weight[0], preferred_element_type=jnp.float32)  6.05 us
    all_to_all x1, waiting for transfers between devices, shards(): lax.all_to_all(mixed, 'tp', split_axis=0, concat_axis=1, tiled=True)  5.96 us
  transfers between devices with their start and end apart: 6, of which 5 were waited for; matrix products, arithmetic and copies ran while one was open for 1% of the time, Pallas kernels for 0%

commit v1 on v0

--- a/solution.py
+++ b/solution.py
@@ -85,7 +85,12 @@
     )
     outgoing = outgoing.astype(jnp.bfloat16).reshape(sp_count, capacity, width)
     arrived = lax.all_to_all(outgoing, "sp", split_axis=0, concat_axis=0, tiled=True)
-    piece = lax.all_gather(arrived, "tp", axis=0, tiled=True)
+    ring = [arrived]
+    for hop in range(3):
+        ring.append(lax.ppermute(ring[-1], "tp", [(dev, (dev + 1) % 4) for dev in range(4)]))
+    piece = jnp.roll(
+        jnp.concatenate(ring[::-1], axis=0), (lax.axis_index("tp") + 1) * ring[0].shape[0], axis=0
+    )
     flat_rows = piece.reshape(-1, width)
     gate_part = jnp.dot(flat_rows, gate_weight[0], preferred_element_type=jnp.float32)
     up_part = jnp.dot(flat_rows, up_weight[0], preferred_element_type=jnp.float32)

time: 248 us -> 277 us (1.12)
  waiting for transfers between devices: 159 us -> 181 us
  local copies, waits for them, and re-layouts: 5 us -> 12.4 us
  matrix products: 22.5 us -> 19.4 us
    ppermute x0 -> x3, waiting for transfers between devices: none -> 72.5 us  [shards(): lax.ppermute(ring[-1], 'tp', [(dev, (dev + 1) % 4) for dev in range(4)])]
    all_gather x1 -> x0, waiting for transfers between devices: 50.4 us -> none  [shards(): piece = lax.all_gather(arrived, 'tp', axis=0, tiled=True)]
    unnamed x18 -> x23, local copies, waits for them, and re-layouts: 2.46 us -> 9.26 us
    dot_general x1, matrix products: 7.49 us -> 4.69 us  [shards(): jnp.dot(flat_rows, up_weight[0], preferred_element_type=jnp.float32)]
  transfers between devices with their start and end apart: 6 -> 8, of which waited for: 5 -> 7; matrix products, arithmetic and copies ran while one was open for 1% -> 1% of each run, Pallas kernels for 0% -> 0%
where the time goes in v1:
time: 277 us
  waiting for transfers between devices  181 us (65%)
  blocking collectives  33.1 us (12%)
  matrix products  19.4 us (7%)
  between operations  13.8 us (5%)
  starting transfers between devices  13.2 us (5%)
  local copies, waits for them, and re-layouts  12.4 us (4%)
  other arithmetic  4.02 us (1%)
    ppermute x3, waiting for transfers between devices, shards(): lax.ppermute(ring[-1], 'tp', [(dev, (dev + 1) % 4) for dev in range(4)])  72.5 us
    reduce_scatter x1, waiting for transfers between devices, shards(): lax.psum_scatter(term.astype(jnp.bfloat16).astype(jnp.float32).astype(jnp...  52.3 us
    all_to_all x1, blocking collectives, shards(): lax.all_to_all(outgoing, 'sp', split_axis=0, concat_axis=0, tiled=True)  33.1 us
    all_to_all x1, waiting for transfers between devices, shards(): lax.all_to_all(expert_out, 'sp', split_axis=0, concat_axis=0, tiled=True)  25.2 us
    all_gather x1, waiting for transfers between devices, shards(): return lax.all_gather(out_own, 'tp', axis=0, tiled=True)  24.6 us
    unnamed x23, local copies, waits for them, and re-layouts  9.26 us
    dot_general x1, matrix products, shards(): jnp.dot(hidden_flat, down_weight[0], preferred_element_type=jnp.float32)  6.05 us
    all_to_all x1, waiting for transfers between devices, shards(): lax.all_to_all(mixed, 'tp', split_axis=0, concat_axis=1, tiled=True)  5.96 us
  transfers between devices with their start and end apart: 8, of which 7 were waited for; matrix products, arithmetic and copies ran while one was open for 1% of the time, Pallas kernels for 0%

profile of v1, /device:TPU:0, one launch (start us, length us, event | category | flops | bytes accessed | tf_op | source)
XLA Modules:
  0.0 276.6 jit_solution(6097891200715248763)
XLA Ops:
  6.5 0.0 copy-start
  6.5 1.5 convert_element_type.65
  8.1 1.5 multiply_reduce_fusion
  9.6 0.8 dynamic_slice.21
  10.4 0.1 multiply_convert_fusion.1
  10.5 2.4 collective-permute-start
  12.9 0.0 copy-done.2
  13.0 0.1 constant_dynamic-slice_fusion.1
  13.0 0.1 copy.17
  13.1 0.1 eq.38
  13.3 0.1 fusion.38
  13.4 0.2 reduce_window_sum.11
  13.5 0.2 select_reduce_fusion
  13.8 0.0 collective-permute-done
  13.8 0.1 maximum_convert_fusion
  13.9 0.0 copy-done
  13.9 0.0 copy-done.6
  13.9 0.0 copy-start.1
  13.9 2.0 fusion.8
  15.9 4.5 %all-to-all-start = ((bf16[4,64,512]{2,1,0:T(8,128)(2,1)}), bf16[4,64,512]{2,1,0:T(8,128)(2,1)S(1)}, u32[]{:S(2)}, u32[]{:S(2)}) async-start(bf16[4,64,512]{2,1,0:T(8,128)(2,1)} %bitcast), calls=%async_computation | async-start | bytes 524288 | tf_op jit(solution)/shard_map/all_to_all | solution.py:74
  20.4 0.0 reduce-scatter.2.cloned.1.call-start
  20.5 6.0 %all-to-all-done = bf16[4,64,512]{2,1,0:T(8,128)(2,1)S(1)} async-done(((bf16[4,64,512]{2,1,0:T(8,128)(2,1)}), bf16[4,64,512]{2,1,0:T(8,128)(2,1)S(1)}, u32[]{:S(2)}, u32[]{:S(2)}) %all-to-all-start) | async-done | bytes 262176 | tf_op jit(solution)/shard_map/all_to_all | solution.py:74
  26.5 0.2 fusion.9
  26.7 0.1 fusion.11
  26.8 0.3 broadcast_in_dim.32
  27.2 0.2 reshape.66
  27.4 0.5 convolution_convert_fusion.1
  27.9 33.1 %all_to_all.23 = bf16[8,32,2048]{2,1,0:T(8,128)(2,1)S(1)} all-to-all(bf16[8,32,2048]{2,1,0:T(8,128)(2,1)S(1)} %bitcast.35), channel_id=1, replica_groups=mesh['sp'=8,'tp'=4] {'sp'}, dimensions={0} | all-to-all | bytes 2097152 | tf_op jit(solution)/shard_map/all_to_all | solution.py:87
  61.0 1.3 collective-permute-start.1
  62.2 24.2 %collective-permute-done.1 = bf16[8,32,2048]{2,1,0:T(8,128)(2,1)S(1)} collective-permute-done((bf16[8,32,2048]{2,1,0:T(8,128)(2,1)S(1)}, bf16[8,32,2048]{2,1,0:T(8,128)(2,1)S(1)}, u32[]{:S(2)}, u32[]{:S(2)}) %collective-permute-start.1) | collective-permute-done | bytes 1048608 | tf_op jit(solution)/shard_map/ppermute | solution.py:90
  86.4 0.4 collective-permute-start.2
  86.8 24.3 %collective-permute-done.2 = bf16[8,32,2048]{2,1,0:T(8,128)(2,1)} collective-permute-done((bf16[8,32,2048]{2,1,0:T(8,128)(2,1)S(1)}, bf16[8,32,2048]{2,1,0:T(8,128)(2,1)}, u32[]{:S(2)}, u32[]{:S(2)}) %collective-permute-start.2) | collective-permute-done | bytes 1048608 | tf_op jit(solution)/shard_map/ppermute | solution.py:90
  111.1 0.0 collective-permute-start.3
  111.1 24.0 %collective-permute-done.3 = bf16[8,32,2048]{2,1,0:T(8,128)(2,1)} collective-permute-done((bf16[8,32,2048]{2,1,0:T(8,128)(2,1)}, bf16[8,32,2048]{2,1,0:T(8,128)(2,1)}, u32[]{:S(2)}, u32[]{:S(2)}) %collective-permute-start.3) | collective-permute-done | bytes 1048608 | tf_op jit(solution)/shard_map/ppermute | solution.py:90
  135.1 1.3 constant_dynamic-update-slice_fusion.7
  136.4 1.3 constant_dynamic-update-slice_fusion.6
  137.7 0.1 constant_dynamic-update-slice_fusion.5
  137.8 0.1 constant_dynamic-update-slice_fusion.4
  137.9 1.3 constant_dynamic-update-slice_fusion.3
  139.2 1.3 constant_dynamic-update-slice_fusion.2
  140.5 0.1 constant_dynamic-update-slice_fusion.1
  140.5 0.1 constant_dynamic-update-slice_fusion
  140.6 0.0 copy-start.3
  140.6 0.6 constant_dynamic-slice_fusion
  141.2 1.4 copy-done.3
  142.7 4.5 %fusion.3 = f32[1024,896]{1,0:T(8,128)S(1)} fusion(bf16[1024,2048]{1,0:T(8,128)(2,1)S(1)} %bitcast.32, bf16[1,2048,896]{2,1,0:T(8,128)(2,1)S(1)} %copy-done.3), kind=kOutput, calls=%fused_computation.4 | convolution fusion | flops 3758096384 | bytes 11534336 | tf_op jit(solution)/shard_map/dot_general | solution.py:95
  147.1 0.0 copy-done.4
  147.2 0.0 copy-start.5
  147.2 4.7 %multiply_convert_fusion = bf16[1024,896]{1,0:T(8,128)(2,1)S(1)} fusion(f32[1024,896]{1,0:T(8,128)S(1)} %fusion.3, bf16[1024,2048]{1,0:T(8,128)(2,1)S(1)} %bitcast.33, bf16[1,2048,896]{2,1,0:T(8,128)(2,1)S(1)} %copy-done.4), kind=kOutput, calls=%fused_computation.6 | convolution fusion | flops 3763601408 | bytes 13369344 | tf_op jit(solution)/shard_map/dot_general | solution.py:96
  151.9 0.0 copy-done.5
  151.9 6.1 %convolution_convert_fusion = bf16[1024,2048]{1,0:T(8,128)(2,1)} fusion(bf16[1024,896]{1,0:T(8,128)(2,1)S(1)} %multiply_convert_fusion, bf16[1,896,2048]{2,1,0:T(8,128)(2,1)S(1)} %copy-done.5), kind=kOutput, calls=%fused_computation | convolution fusion | flops 3760193536 | bytes 9699328 | tf_op jit(solution)/shard_map/dot_general | solution.py:100
  157.9 0.0 reduce-scatter.2.cloned.1.call-update
  157.9 52.3 %reduce-scatter.2.cloned.1.call-done = bf16[256,2048]{1,0:T(8,128)(2,1)} async-done(((bf16[1024,2048]{1,0:T(8,128)(2,1)}), bf16[256,2048]{1,0:T(8,128)(2,1)}) %reduce-scatter.2.cloned.1.call-update) | async-done | bytes 1048592 | tf_op jit(solution)/shard_map/reduce_scatter | solution.py:101
  210.2 4.6 %all-to-all-start.2 = ((bf16[8,32,2048]{2,1,0:T(8,128)(2,1)}), bf16[8,32,2048]{2,1,0:T(8,128)(2,1)S(1)}, u32[]{:S(2)}, u32[]{:S(2)}) async-start(bf16[8,32,2048]{2,1,0:T(8,128)(2,1)} %bitcast.37), calls=%async_computation.3 | async-start | bytes 2097152 | tf_op jit(solution)/shard_map/all_to_all | solution.py:108
  214.9 0.0 all-gather.2.cloned.1.call-start
  214.9 0.1 reduce_sum.31
  215.0 0.8 fusion.39
  215.8 0.1 copy.15
  215.9 0.3 fusion.30
  216.2 25.2 %all-to-all-done.2 = bf16[8,32,2048]{2,1,0:T(8,128)(2,1)S(1)} async-done(((bf16[8,32,2048]{2,1,0:T(8,128)(2,1)}), bf16[8,32,2048]{2,1,0:T(8,128)(2,1)S(1)}, u32[]{:S(2)}, u32[]{:S(2)}) %all-to-all-start.2) | async-done | bytes 1048608 | tf_op jit(solution)/shard_map/all_to_all | solution.py:108
  241.4 1.4 fusion.5
  242.8 0.0 all-gather.2.cloned.1.call-update
  242.8 24.6 %all-gather.2.cloned.1.call-done = bf16[256,2048]{1,0:T(8,128)(2,1)} async-done(((bf16[64,2048]{1,0:T(8,128)(2,1)}), bf16[256,2048]{1,0:T(8,128)(2,1)}) %all-gather.2.cloned.1.call-update) | async-done | bytes 1048592 | tf_op jit(solution)/shard_map/all_gather | solution.py:119
  267.4 2.3 copy.31
  (12 shorter events, 0.1 us)
Async XLA Ops:
  6.5 7.3 %copy-start = (bf16[512,512]{1,0:T(8,128)(2,1)S(1)}, bf16[512,512]{1,0:T(8,128)(2,1)}, u32[]{:S(2)}) copy-start(bf16[512,512]{1,0:T(8,128)(2,1)} %param.12) | copy-start | bytes 1572868
  6.5 6.4 %copy-start.2 = (s32[256,2]{0,1:T(2,128)S(1)}, s32[256,2]{0,1:T(2,128)}, u32[]{:S(2)}) copy-start(s32[256,2]{0,1:T(2,128)} %param.15) | copy-start | bytes 6148
  6.5 7.3 %copy-start.6 = (f32[512]{0:T(512)S(1)}, f32[512]{0:T(512)}, u32[]{:S(2)}) copy-start(f32[512]{0:T(512)} %param.13) | copy-start | bytes 6148
  10.5 3.3 %collective-permute-start = (bf16[16,512]{1,0:T(8,128)(2,1)S(1)}, bf16[16,512]{1,0:T(8,128)(2,1)S(1)}, u32[]{:S(2)}, u32[]{:S(2)}) collective-permute-start(bf16[16,512]{1,0:T(8,128)(2,1)S(1)} %slice.69), channel_id=1, source_target_pairs={{0,4},{4,8},{8,12},{12,16},{16,20},{20,24},{24,28},{1,5},{5,9},{9,... | collective-permute-start | bytes 49160 | tf_op jit(solution)/shard_map/ppermute | solution.py:15
  13.9 12.8 %copy-start.1 = (f32[2048]{0:T(1024)S(1)}, f32[2048]{0:T(1024)}, u32[]{:S(2)}) copy-start(f32[2048]{0:T(1024)} %param.14) | copy-start | bytes 24580
  15.9 10.5 %all-to-all-start = ((bf16[4,64,512]{2,1,0:T(8,128)(2,1)}), bf16[4,64,512]{2,1,0:T(8,128)(2,1)S(1)}, u32[]{:S(2)}, u32[]{:S(2)}) async-start(bf16[4,64,512]{2,1,0:T(8,128)(2,1)} %bitcast), calls=%async_computation | async-start | bytes 524288 | tf_op jit(solution)/shard_map/all_to_all | solution.py:74
  20.4 189.8 %reduce-scatter.2.cloned.1.call-start = ((), (), s32[]{:S(2)}) async-start(), calls=%async_computation.4 | async-start | bytes 5242880 | tf_op jit(solution)/shard_map/reduce_scatter | solution.py:101
  61.0 25.4 %collective-permute-start.1 = (bf16[8,32,2048]{2,1,0:T(8,128)(2,1)S(1)}, bf16[8,32,2048]{2,1,0:T(8,128)(2,1)S(1)}, u32[]{:S(2)}, u32[]{:S(2)}) collective-permute-start(bf16[8,32,2048]{2,1,0:T(8,128)(2,1)S(1)} %all_to_all.23), channel_id=1, source_target_pairs={{0,1},{1,2},{2,3},{3,0},{4,5},{5,6},{6,7},{7,4},{8,9},{9,10},{10,1... | collective-permute-start | bytes 3145736 | tf_op jit(solution)/shard_map/ppermute | solution.py:90
  86.4 24.7 %collective-permute-start.2 = (bf16[8,32,2048]{2,1,0:T(8,128)(2,1)S(1)}, bf16[8,32,2048]{2,1,0:T(8,128)(2,1)}, u32[]{:S(2)}, u32[]{:S(2)}) collective-permute-start(bf16[8,32,2048]{2,1,0:T(8,128)(2,1)S(1)} %collective-permute-done.1), channel_id=1, source_target_pairs={{0,1},{1,2},{2,3},{3,0},{4,5},{5,6},{6,7},{7,4},{8,9},{9,10},{10,1... | collective-permute-start | bytes 3145736 | tf_op jit(solution)/shard_map/ppermute | solution.py:90
  111.1 24.0 %collective-permute-start.3 = (bf16[8,32,2048]{2,1,0:T(8,128)(2,1)}, bf16[8,32,2048]{2,1,0:T(8,128)(2,1)}, u32[]{:S(2)}, u32[]{:S(2)}) collective-permute-start(bf16[8,32,2048]{2,1,0:T(8,128)(2,1)} %collective-permute-done.2), channel_id=1, source_target_pairs={{0,1},{1,2},{2,3},{3,0},{4,5},{5,6},{6,7},{7,4},{8,9},{9,10},{10,1... | collective-permute-start | bytes 3145736 | tf_op jit(solution)/shard_map/ppermute | solution.py:90
  140.6 2.0 copy-start.3
  142.7 4.5 %copy-start.4 = (bf16[1,2048,896]{2,1,0:T(8,128)(2,1)S(1)}, bf16[1,2048,896]{2,1,0:T(8,128)(2,1)}, u32[]{:S(2)}) copy-start(bf16[1,2048,896]{2,1,0:T(8,128)(2,1)} %param.18) | copy-start | bytes 11010052
  147.2 4.7 %copy-start.5 = (bf16[1,896,2048]{2,1,0:T(8,128)(2,1)S(1)}, bf16[1,896,2048]{2,1,0:T(8,128)(2,1)}, u32[]{:S(2)}) copy-start(bf16[1,896,2048]{2,1,0:T(8,128)(2,1)} %param.19) | copy-start | bytes 11010052
  210.2 31.2 %all-to-all-start.2 = ((bf16[8,32,2048]{2,1,0:T(8,128)(2,1)}), bf16[8,32,2048]{2,1,0:T(8,128)(2,1)S(1)}, u32[]{:S(2)}, u32[]{:S(2)}) async-start(bf16[8,32,2048]{2,1,0:T(8,128)(2,1)} %bitcast.37), calls=%async_computation.3 | async-start | bytes 2097152 | tf_op jit(solution)/shard_map/all_to_all | solution.py:108
  214.9 52.6 %all-gather.2.cloned.1.call-start = ((), (), s32[]{:S(2)}) async-start(), calls=%async_computation.5 | async-start | bytes 1310720 | tf_op jit(solution)/shard_map/all_gather | solution.py:119
Sparse Core Ops, SparseCore 0:
  158.1 52.1 reduce-scatter.1
  242.9 24.4 all-gather.1
